TPU v7x, 32 devices: a whole 2x2x4 slice. The times are simulated.
32 devices in a mesh: grp: 2 (over y), fs: 4 (over z), tp: 4 (over x, core).
Axes of the slice: x: 2, y: 2, z: 4, core: 2. Of those that a mesh axis runs over, the one named last changes fastest.
Arguments:
- tokens: bfloat16 [1024, 2048], P(('grp', 'fs')), parts along dimension 0, may hold values from -12 to 12, as said below
- mix_heads: bfloat16 [1024, 2048], P(('grp', 'fs'), 'tp'), parts along dimension 0, may hold values from -6 to 6
- norm_first: float32 [2048], replicated, may hold values from 0.1 to 1.9
- gate_first: bfloat16 [2048, 5632], P('fs', 'tp'), may hold values from -0.125 to 0.125
- up_first: bfloat16 [2048, 5632], P('fs', 'tp'), may hold values from -0.125 to 0.125
- down_first: bfloat16 [5632, 2048], P('tp', 'fs'), may hold values from -0.078125 to 0.078125
- out_weight: bfloat16 [2048, 2048], P('tp', 'fs'), may hold values from -0.125 to 0.125
- norm_second: float32 [2048], replicated, may hold values from 0.1 to 1.9
- gate_second: bfloat16 [2048, 5632], P('fs', 'tp'), may hold values from -0.125 to 0.125
- up_second: bfloat16 [2048, 5632], P('fs', 'tp'), may hold values from -0.125 to 0.125
- down_second: bfloat16 [5632, 2048], P('tp', 'fs'), may hold values from -0.078125 to 0.078125
Outputs:
- layer_out: bfloat16 [1024, 2048], P(('grp', 'fs')), parts along dimension 0
There are 2 independent parts, one for each index of `grp`. A program takes and returns all parts, laid end to end along the dimension named above; an argument that names none is the same for every part. Nothing has to cross between parts.
Inputs may be any that keep to these rules, and one draw needn't show every extreme that they name: Each row of tokens carries a scale of its own.
All inputs are finite; a program needn't handle non-finite values.
Results may differ from a plain program's by a relative error of at most 0.014.
Values may be sent and summed in bfloat16 or wider, within the bound.
A program may use at most 64 MiB of HBM per device.

v0:
```python
import jax
import jax.numpy as jnp
from jax import lax
from jax.sharding import PartitionSpec as P

EPS = 0.1


def norm_rows(row_block, gain_vector):
    widened = row_block.astype(jnp.float32)
    scaled = widened * lax.rsqrt(jnp.mean(widened * widened, axis=-1, keepdims=True) + EPS)
    return (scaled * gain_vector).astype(jnp.bfloat16)


def gate_values(normed, gate_weight, value_weight):
    whole_gate, whole_values = (
        lax.all_gather(gate_weight, "fs", axis=0, tiled=True),
        lax.all_gather(value_weight, "fs", axis=0, tiled=True),
    )
    return (
        jnp.dot(normed, whole_gate, preferred_element_type=jnp.float32),
        jnp.dot(normed, whole_values, preferred_element_type=jnp.float32),
    )


def half_branch(normed, gate_weight, value_weight, down_weight):
    gates, values = gate_values(normed, gate_weight, value_weight)
    hidden = (jax.nn.silu(gates) * values).astype(jnp.bfloat16)
    return 0.5 * jnp.dot(
        hidden,
        lax.all_gather(down_weight, "fs", axis=1, tiled=True),
        preferred_element_type=jnp.float32,
    )


def share_sum(block_terms):
    return lax.psum_scatter(
        block_terms.astype(jnp.bfloat16), "tp", scatter_dimension=0, tiled=True
    ).astype(jnp.float32)


def join_rows(row_block):
    return lax.all_gather(row_block, "tp", axis=0, tiled=True)


def local(
    tokens,
    mix_heads,
    norm_first,
    gate_first,
    up_first,
    down_first,
    out_weight,
    norm_second,
    gate_second,
    up_second,
    down_second,
):
    normed_one = norm_rows(tokens, norm_first)
    first_terms = half_branch(normed_one, gate_first, up_first, down_first)
    heads_out = jnp.dot(
        mix_heads,
        lax.all_gather(out_weight, "fs", axis=1, tiled=True),
        preferred_element_type=jnp.float32,
    )
    first_terms = first_terms + heads_out
    share_rows = tokens.shape[0] // lax.axis_size("tp")
    offset = lax.axis_index("tp") * share_rows
    own_rows = lax.dynamic_slice_in_dim(tokens, offset, share_rows, 0).astype(jnp.float32)
    resid_two = own_rows + share_sum(first_terms)
    normed_two = join_rows(norm_rows(resid_two, norm_second))
    second_terms = half_branch(normed_two, gate_second, up_second, down_second)
    finished = (resid_two + share_sum(second_terms)).astype(jnp.bfloat16)
    return join_rows(finished)


def solution(mesh):
    in_specs = (
        P(("grp", "fs"), None),
        P(("grp", "fs"), "tp"),
        P(),
        P("fs", "tp"),
        P("fs", "tp"),
        P("tp", "fs"),
        P("tp", "fs"),
        P(),
        P("fs", "tp"),
        P("fs", "tp"),
        P("tp", "fs"),
    )
    out_specs = P(("grp", "fs"), None)
    return jax.shard_map(local, mesh=mesh, in_specs=in_specs, out_specs=out_specs, check_vma=False)
```

profile of v0, /device:TPU:26, one launch (start us, length us, event | category | flops | bytes accessed | tf_op | source)
XLA Modules:
  0.0 761.4 jit_solution(13067139635178607233)
XLA Ops:
  6.5 0.0 copy-start
  6.5 0.0 all-gather.8.cloned.1.call-start
  6.5 0.7 all-gather.8.cloned.1.call-update
  7.3 0.0 copy-start.1
  7.3 0.0 copy-start.3
  7.3 0.0 all-gather.10.cloned.1.call-start
  7.3 0.7 all-gather.10.cloned.1.call-update
  8.0 0.0 all-gather.12.cloned.1.call-start
  8.1 0.7 all-gather.12.cloned.1.call-update
  8.8 0.0 all-gather.14.cloned.1.call-start
  8.8 0.5 all-gather.14.cloned.1.call-update
  9.3 0.0 reduce-scatter.3.cloned.1.call-start
  9.4 1.2 fusion.4
  10.6 103.2 %all-gather.8.cloned.1.call-done = bf16[2048,1408]{1,0:T(8,128)(2,1)} async-done(((bf16[512,1408]{1,0:T(8,128)(2,1)}), bf16[2048,1408]{1,0:T(8,128)(2,1)}) %all-gather.8.cloned.1.call-update) | async-done | bytes 5767184 | tf_op jit(solution)/shard_map/all_gather | solution.py:17
  113.8 3.9 fusion.11
  117.7 102.7 %all-gather.10.cloned.1.call-done = bf16[2048,1408]{1,0:T(8,128)(2,1)} async-done(((bf16[512,1408]{1,0:T(8,128)(2,1)}), bf16[2048,1408]{1,0:T(8,128)(2,1)}) %all-gather.10.cloned.1.call-update) | async-done | bytes 5767184 | tf_op jit(solution)/shard_map/all_gather | solution.py:18
  220.4 106.5 %all-gather.12.cloned.1.call-done = bf16[1408,2048]{1,0:T(8,128)(2,1)} async-done(((bf16[1408,512]{1,0:T(8,128)(2,1)}), bf16[1408,2048]{1,0:T(8,128)(2,1)}) %all-gather.12.cloned.1.call-update) | async-done | bytes 5767184 | tf_op jit(solution)/shard_map/all_gather | solution.py:31
  326.9 0.0 copy-done.1
  326.9 0.0 copy-done.3
  326.9 6.3 convolution_multiply_fusion.3
  333.2 0.0 copy-start.4
  333.2 39.7 %all-gather.14.cloned.1.call-done = bf16[512,2048]{1,0:T(8,128)(2,1)} async-done(((bf16[512,512]{1,0:T(8,128)(2,1)}), bf16[512,2048]{1,0:T(8,128)(2,1)}) %all-gather.14.cloned.1.call-update) | async-done | bytes 2097168 | tf_op jit(solution)/shard_map/all_gather | solution.py:63
  372.9 0.0 copy-done
  372.9 2.8 fusion
  375.7 0.0 reduce-scatter.3.cloned.1.call-update
  375.8 0.0 all-gather.16.cloned.1.call-start
  375.8 0.5 all-gather.16.cloned.1.call-update
  376.3 0.0 all-gather.18.cloned.1.call-start
  376.4 0.7 all-gather.18.cloned.1.call-update
  377.1 0.0 all-gather.20.cloned.1.call-start
  377.1 0.7 all-gather.20.cloned.1.call-update
  377.8 0.0 reduce-scatter.5.cloned.1.call-start
  377.9 19.7 %reduce-scatter.3.cloned.1.call-done = bf16[32,2048]{1,0:T(8,128)(2,1)} async-done(((bf16[128,2048]{1,0:T(8,128)(2,1)}), bf16[32,2048]{1,0:T(8,128)(2,1)}) %reduce-scatter.3.cloned.1.call-update) | async-done | bytes 131088 | tf_op jit(solution)/shard_map/reduce_scatter | solution.py:37
  397.6 1.1 multiply_reduce_fusion
  398.7 0.0 copy-done.4
  398.7 1.0 multiply_convert_fusion
  399.7 7.2 all_gather.31
  406.9 97.1 %all-gather.16.cloned.1.call-done = bf16[2048,1408]{1,0:T(8,128)(2,1)} async-done(((bf16[512,1408]{1,0:T(8,128)(2,1)}), bf16[2048,1408]{1,0:T(8,128)(2,1)}) %all-gather.16.cloned.1.call-update) | async-done | bytes 5767184 | tf_op jit(solution)/shard_map/all_gather | solution.py:17
  503.9 3.6 fusion.15
  507.6 0.0 copy-start.2
  507.6 102.9 %all-gather.18.cloned.1.call-done = bf16[2048,1408]{1,0:T(8,128)(2,1)} async-done(((bf16[512,1408]{1,0:T(8,128)(2,1)}), bf16[2048,1408]{1,0:T(8,128)(2,1)}) %all-gather.18.cloned.1.call-update) | async-done | bytes 5767184 | tf_op jit(solution)/shard_map/all_gather | solution.py:18
  610.5 106.5 %all-gather.20.cloned.1.call-done = bf16[1408,2048]{1,0:T(8,128)(2,1)} async-done(((bf16[1408,512]{1,0:T(8,128)(2,1)}), bf16[1408,2048]{1,0:T(8,128)(2,1)}) %all-gather.20.cloned.1.call-update) | async-done | bytes 5767184 | tf_op jit(solution)/shard_map/all_gather | solution.py:31
  717.0 7.1 fusion.1
  724.1 0.0 reduce-scatter.5.cloned.1.call-update
  724.1 21.9 %reduce-scatter.5.cloned.1.call-done = bf16[32,2048]{1,0:T(8,128)(2,1)} async-done(((bf16[128,2048]{1,0:T(8,128)(2,1)}), bf16[32,2048]{1,0:T(8,128)(2,1)}) %reduce-scatter.5.cloned.1.call-update) | async-done | bytes 131088 | tf_op jit(solution)/shard_map/reduce_scatter | solution.py:37
  746.0 0.0 copy-done.2
  746.0 1.0 add_convert_fusion
  747.0 7.1 all_gather.35
  754.1 0.8 copy.13
  (2 shorter events, 0.0 us)
Async XLA Ops:
  6.5 366.4 %copy-start = (bf16[128,512]{1,0:T(8,128)(2,1)S(1)}, bf16[128,512]{1,0:T(8,128)(2,1)}, u32[]{:S(2)}) copy-start(bf16[128,512]{1,0:T(8,128)(2,1)} %param.12) | copy-start | bytes 393220
  6.5 107.3 %all-gather.8.cloned.1.call-start = ((), (), s32[]{:S(2)}) async-start(), calls=%async_computation.2 | async-start | bytes 7208960 | tf_op jit(solution)/shard_map/all_gather | solution.py:17
  7.3 319.7 %copy-start.1 = (bf16[128,2048]{1,0:T(8,128)(2,1)S(1)}, bf16[128,2048]{1,0:T(8,128)(2,1)}, u32[]{:S(2)}) copy-start(bf16[128,2048]{1,0:T(8,128)(2,1)} %param.11) | copy-start | bytes 1572868
  7.3 319.7 %copy-start.3 = (f32[2048]{0:T(1024)S(1)}, f32[2048]{0:T(1024)}, u32[]{:S(2)}) copy-start(f32[2048]{0:T(1024)} %param.13) | copy-start | bytes 24580
  7.3 213.1 %all-gather.10.cloned.1.call-start = ((), (), s32[]{:S(2)}) async-start(), calls=%async_computation.3 | async-start | bytes 7208960 | tf_op jit(solution)/shard_map/all_gather | solution.py:18
  8.0 318.9 %all-gather.12.cloned.1.call-start = ((), (), s32[]{:S(2)}) async-start(), calls=%async_computation.4 | async-start | bytes 7208960 | tf_op jit(solution)/shard_map/all_gather | solution.py:31
  8.8 364.1 %all-gather.14.cloned.1.call-start = ((), (), s32[]{:S(2)}) async-start(), calls=%async_computation.5 | async-start | bytes 2621440 | tf_op jit(solution)/shard_map/all_gather | solution.py:63
  9.3 388.3 %reduce-scatter.3.cloned.1.call-start = ((), (), s32[]{:S(2)}) async-start(), calls=%async_computation.6 | async-start | bytes 655360 | tf_op jit(solution)/shard_map/reduce_scatter | solution.py:37
  333.2 65.5 %copy-start.4 = (f32[2048]{0:T(1024)S(1)}, f32[2048]{0:T(1024)}, u32[]{:S(2)}) copy-start(f32[2048]{0:T(1024)} %param.18) | copy-start | bytes 24580
  375.8 128.2 %all-gather.16.cloned.1.call-start = ((), (), s32[]{:S(2)}) async-start(), calls=%async_computation.7 | async-start | bytes 7208960 | tf_op jit(solution)/shard_map/all_gather | solution.py:17
  376.3 234.1 %all-gather.18.cloned.1.call-start = ((), (), s32[]{:S(2)}) async-start(), calls=%async_computation.8 | async-start | bytes 7208960 | tf_op jit(solution)/shard_map/all_gather | solution.py:18
  377.1 339.9 %all-gather.20.cloned.1.call-start = ((), (), s32[]{:S(2)}) async-start(), calls=%async_computation.9 | async-start | bytes 7208960 | tf_op jit(solution)/shard_map/all_gather | solution.py:31
  377.8 368.2 %reduce-scatter.5.cloned.1.call-start = ((), (), s32[]{:S(2)}) async-start(), calls=%async_computation.10 | async-start | bytes 655360 | tf_op jit(solution)/shard_map/reduce_scatter | solution.py:37
  507.6 238.4 %copy-start.2 = (bf16[32,2048]{1,0:T(8,128)(2,1)S(1)}, bf16[32,2048]{1,0:T(8,128)(2,1)}, u32[]{:S(2)}) copy-start(bf16[32,2048]{1,0:T(8,128)(2,1)} %reduce-scatter.3.cloned.1.call-done) | copy-start | bytes 393220
Sparse Core Ops, SparseCore 0:
  8.9 104.8 all-gather.7
  115.4 104.9 all-gather.9
  222.0 104.9 all-gather.11
  328.4 44.4 all-gather.13
  375.9 21.6 reduce-scatter.2
  399.1 104.8 all-gather.15
  505.5 104.9 all-gather.17
  612.1 104.9 all-gather.19
  724.2 21.7 reduce-scatter.4
where the time goes:
time: 764 us; the launch traced here: 761 us
  waiting for transfers between devices  705 us (92%)
  matrix products  23.6 us (3%)
  blocking collectives  14.3 us (2%)
  between operations  13.3 us (2%)
    all_gather x2, waiting for transfers between devices, half_branch(): lax.all_gather(down_weight, 'fs', axis=1, tiled=True)  213 us
    all_gather x2, waiting for transfers between devices, gate_values(): lax.all_gather(value_weight, 'fs', axis=0, tiled=True)  206 us
    all_gather x2, waiting for transfers between devices, gate_values(): lax.all_gather(gate_weight, 'fs', axis=0, tiled=True)  200 us
    reduce_scatter x2, waiting for transfers between devices, share_sum(): lax.psum_scatter(block_terms.astype(jnp.bfloat16), 'tp', scatter_dimensio...  41.6 us
    all_gather x1, waiting for transfers between devices, local(): lax.all_gather(out_weight, 'fs', axis=1, tiled=True)  39.7 us
  transfers between devices with their start and end apart: 9, of which 9 were waited for; matrix products, arithmetic and copies ran while one was open for 2% of the time, Pallas kernels for 0%

commit v1 on v0

v1 whole, which is shorter than its diff:
```python
import functools

import jax
import jax.numpy as jnp
from jax import lax
from jax.experimental import pallas as pl
from jax.experimental.pallas import tpu as pltpu
from jax.sharding import PartitionSpec as P

EPS = 0.1
MESH = pl.DeviceIdType.MESH
BF16 = jnp.bfloat16
F32 = jnp.float32


def loop(count, body):
    def step(i, carry):
        body(i)
        return carry

    lax.fori_loop(0, count, step, 0)


def kernel(n_fs, n_tp, chunk,
           tok, mix, gain1, wg1, wu1, wd1, wo, gain2, wg2, wu2, wd2,
           out,
           vg1, vu1, vd1, vo, vg2, vu2, vd2,
           norm_rows, raw, nb1, nb2, mixed, grads, sums, in1, in2, hid1, hid2,
           terms, got1, got2, resid, squares, done_rows, joined,
           wsem, p0_send, p0_recv, raw_send, raw_recv, mix_send, mix_recv,
           rs_send, rs_recv, ag_send, ag_recv, tp_send, tp_recv,
           sq_send, sq_recv, nrm_send, nrm_recv, out_send, out_recv):
    f, t = lax.axis_index("fs"), lax.axis_index("tp")
    rows_in, width = tok.shape
    total = rows_in * n_fs
    share = total // n_tp
    half = total // 2
    n_chunks = half // chunk
    dc = width // n_fs

    weights = ((wg1, vg1), (wu1, vu1), (wd1, vd1), (wo, vo), (wg2, vg2), (wu2, vu2), (wd2, vd2))
    loads = [pltpu.make_async_copy(a, b, wsem.at[i]) for i, (a, b) in enumerate(weights)]
    for load in loads:
        load.start()

    barrier = pltpu.get_barrier_semaphore()

    def greet(i):
        pf, pt = i // n_tp, i % n_tp

        @pl.when(jnp.logical_or(pf != f, pt != t))
        def _():
            pl.semaphore_signal(barrier, inc=1, device_id={"fs": pf, "tp": pt}, device_id_type=MESH)

    loop(n_fs * n_tp, greet)

    def cols(j):
        return pl.ds(pl.multiple_of(j * dc, dc), dc)

    def block(j, size):
        return pl.ds(pl.multiple_of(j * size, size), size)

    def remote(src, dst, send, recv, **where):
        return pltpu.make_async_remote_copy(
            src_ref=src, dst_ref=dst, send_sem=send, recv_sem=recv,
            device_id=where, device_id_type=MESH)

    def norm_piece(i):
        rows = block(i, 32)
        x = tok[rows, :].astype(F32)
        scaled = x * lax.rsqrt(jnp.mean(x * x, axis=-1, keepdims=True) + EPS)
        norm_rows[rows, :] = (scaled * gain1[...]).astype(BF16)

    loop(rows_in // 32, norm_piece)
    pl.semaphore_wait(barrier, n_fs * n_tp - 1)

    def p0_copy(j, slot):
        return remote(norm_rows.at[:, cols(j)], nb1.at[block(slot, rows_in), :],
                      p0_send.at[j], p0_recv.at[slot], fs=j)

    def raw_copy(j):
        return remote(tok.at[:, cols(j)], raw, raw_send.at[j], raw_recv, fs=j)

    def mix_copy(slot, side, where):
        place = mixed.at[block(slot, rows_in), :]
        return remote(place, place, mix_send.at[slot, side], mix_recv.at[slot], fs=where)

    def p0_start(i):
        j = (f + 1 + i) % n_fs
        p0_copy(j, f).start()

    loop(n_fs - 1, p0_start)
    nb1[block(f, rows_in), :] = norm_rows[:, cols(f)]
    mixed[block(f, rows_in), :] = mix[...]

    @pl.when(f == t)
    def _():
        def raw_start(i):
            raw_copy((f + 1 + i) % n_fs).start()

        loop(n_fs - 1, raw_start)
        raw[...] = tok[:, cols(f)]

    def gates(nb, vg, vu, before):
        def piece(i):
            j = (f + i) % n_fs
            before(j)
            rows = block(j, rows_in)
            x = nb[rows, :]
            grads[0, rows, :] = jnp.dot(x, vg[...], preferred_element_type=F32)
            grads[1, rows, :] = jnp.dot(x, vu[...], preferred_element_type=F32)

        loop(n_fs, piece)

    def chain(layer, arrived, hid, with_mix):
        def side_of(side):
            hops = (n_fs - 1 - f) if side == 0 else f
            toward = (f - 1) if side == 0 else (f + 1)
            away = (f + 1) if side == 0 else (f - 1)
            return hops, toward, away

        def rows_of(side, c):
            return pl.ds(pl.multiple_of(side * half + c * chunk, chunk), chunk)

        def rs_copy(side, c, where):
            rows = rows_of(side, c)
            return remote(sums.at[:, rows, :], arrived.at[:, rows, :],
                          rs_send.at[layer, side, c], rs_recv.at[layer, side, c], fs=where)

        def ag_copy(side, c, where):
            rows = rows_of(side, c)
            return remote(hid.at[rows, :], hid.at[rows, :],
                          ag_send.at[layer, side, c], ag_recv.at[layer, side, c], fs=where)

        def step(s):
            for side in (0, 1):
                hops, toward, away = side_of(side)
                c = s - hops

                @pl.when(jnp.logical_and(c >= 0, c < n_chunks))
                def _():
                    rows = rows_of(side, c)

                    @pl.when(hops == 0)
                    def _():
                        sums[:, rows, :] = grads[:, rows, :].astype(BF16)
                        rs_copy(side, c, toward).start()

                    @pl.when(hops > 0)
                    def _():
                        rs_copy(side, c, f).wait_recv()

                    @pl.when(jnp.logical_and(hops > 0, hops < n_fs - 1))
                    def _():
                        sums[:, rows, :] = (grads[:, rows, :] + arrived[:, rows, :].astype(F32)).astype(BF16)
                        rs_copy(side, c, toward).start()

                    @pl.when(hops == n_fs - 1)
                    def _():
                        g = grads[0, rows, :] + arrived[0, rows, :].astype(F32)
                        v = grads[1, rows, :] + arrived[1, rows, :].astype(F32)
                        hid[rows, :] = (g / (1.0 + jnp.exp(-g)) * v).astype(BF16)
                        ag_copy(side, c, away).start()

            for side in (0, 1):
                hops, toward, away = side_of(side)
                dist = n_fs - 1 - hops
                c = s - (n_fs - 1) - dist

                @pl.when(jnp.logical_and(dist > 0, jnp.logical_and(c >= 0, c < n_chunks)))
                def _():
                    ag_copy(side, c, f).wait_recv()

                    @pl.when(dist < n_fs - 1)
                    def _():
                        ag_copy(side, c, away).start()

            if with_mix:
                @pl.when(s < n_fs)
                def _():
                    low, high = f - s, f + s

                    @pl.when(low >= 0)
                    def _():
                        @pl.when(s > 0)
                        def _():
                            mix_copy(low, 0, f).wait_recv()

                        @pl.when(f < n_fs - 1)
                        def _():
                            mix_copy(low, 0, f + 1).start()

                    @pl.when(high < n_fs)
                    def _():
                        @pl.when(s > 0)
                        def _():
                            mix_copy(high, 1, f).wait_recv()

                        @pl.when(f > 0)
                        def _():
                            mix_copy(high, 1, f - 1).start()

        loop(n_chunks + 2 * (n_fs - 1), step)

        def drain(c):
            for side in (0, 1):
                hops, toward, away = side_of(side)

                @pl.when(hops < n_fs - 1)
                def _():
                    rs_copy(side, c, f).wait_send()

                @pl.when(hops > 0)
                def _():
                    ag_copy(side, c, f).wait_send()

        loop(n_chunks, drain)

    def tp_copy(layer, j, slot, got):
        return remote(terms.at[block(j, share), :], got.at[slot],
                      tp_send.at[layer, j], tp_recv.at[layer, slot], tp=j)

    def reduce_tp(layer, hid, vd, got, start_value, with_mix):
        def piece(i):
            j = (t + 1 + i) % n_tp
            rows = block(j, share)
            value = 0.5 * jnp.dot(hid[rows, :], vd[...], preferred_element_type=F32)
            if with_mix:
                value = value + jnp.dot(mixed[rows, :], vo[...], preferred_element_type=F32)
            terms[rows, :] = value.astype(BF16)

            @pl.when(i < n_tp - 1)
            def _():
                tp_copy(layer, j, t, got).start()

        loop(n_tp, piece)
        resid[...] = start_value + terms[block(t, share), :].astype(F32)

        def add(i):
            j = (t + 1 + i) % n_tp
            tp_copy(layer, j, j, got).wait_recv()
            resid[...] = resid[...] + got[j].astype(F32)

        loop(n_tp - 1, add)

        def drain(i):
            j = (t + 1 + i) % n_tp
            tp_copy(layer, j, t, got).wait_send()

        loop(n_tp - 1, drain)

    loads[0].wait()
    loads[1].wait()

    def need_rows(j):
        @pl.when(j != f)
        def _():
            p0_copy(j, j).wait_recv()

    gates(nb1, vg1, vu1, need_rows)
    chain(0, in1, hid1, True)
    loads[2].wait()
    loads[3].wait()

    @pl.when(f != t)
    def _():
        raw_copy(f).wait_recv()

    reduce_tp(0, hid1, vd1, got1, raw[...].astype(F32), True)

    def sq_copy(j, slot):
        return remote(squares.at[f], squares.at[slot], sq_send.at[j], sq_recv.at[slot], fs=j)

    x = resid[...]
    own = jnp.sum(x * x, axis=-1, keepdims=True)
    squares[f] = jnp.transpose(jnp.broadcast_to(own, (share, 128)))[0:8, :]

    def sq_start(i):
        sq_copy((f + 1 + i) % n_fs, f).start()

    def sq_wait(i):
        j = (f + 1 + i) % n_fs
        sq_copy(j, j).wait_recv()

    loop(n_fs - 1, sq_start)
    loop(n_fs - 1, sq_wait)
    summed = squares[0]
    for j in range(1, n_fs):
        summed = summed + squares[j]
    mean = jnp.transpose(jnp.broadcast_to(summed[0:1, :], (128, share)))[:, 0:1] * (1.0 / width)
    nb2[block(t, share), :] = (resid[...] * lax.rsqrt(mean + EPS) * gain2[:, cols(f)]).astype(BF16)

    def nrm_copy(j, slot):
        place = nb2.at[block(slot, share), :]
        return remote(place, place, nrm_send.at[j], nrm_recv.at[slot], tp=j)

    def nrm_start(i):
        nrm_copy((t + 1 + i) % n_tp, t).start()

    def nrm_wait(i):
        j = (t + 1 + i) % n_tp
        nrm_copy(j, j).wait_recv()

    loop(n_tp - 1, nrm_start)
    loads[4].wait()
    loads[5].wait()
    loop(n_tp - 1, nrm_wait)
    gates(nb2, vg2, vu2, lambda j: None)
    chain(1, in2, hid2, False)
    loads[6].wait()
    reduce_tp(1, hid2, vd2, got2, resid[...], False)
    done_rows[...] = resid[...].astype(BF16)

    def out_copy(j, slot):
        return remote(done_rows, joined.at[:, cols(slot)], out_send.at[j], out_recv.at[slot], fs=t, tp=j)

    def out_start(i):
        j = (t + i) % n_tp

        @pl.when(jnp.logical_or(f != t, j != t))
        def _():
            out_copy(j, f).start()

    loop(n_tp, out_start)

    @pl.when(f == t)
    def _():
        joined[:, cols(f)] = done_rows[...]

    def out_wait(j):
        @pl.when(jnp.logical_or(f != t, j != f))
        def _():
            out_copy(t, j).wait_recv()

    loop(n_fs, out_wait)
    out[...] = joined[...]

    def last_fs(i):
        j = (f + 1 + i) % n_fs
        p0_copy(j, f).wait_send()
        sq_copy(j, f).wait_send()

        @pl.when(f == t)
        def _():
            raw_copy(j).wait_send()

    loop(n_fs - 1, last_fs)

    def last_mix(j):
        @pl.when(jnp.logical_and(j <= f, f < n_fs - 1))
        def _():
            mix_copy(j, 0, f).wait_send()

        @pl.when(jnp.logical_and(j >= f, f > 0))
        def _():
            mix_copy(j, 1, f).wait_send()

    loop(n_fs, last_mix)

    def last_tp(i):
        nrm_copy((t + 1 + i) % n_tp, t).wait_send()

    loop(n_tp - 1, last_tp)

    def last_out(j):
        @pl.when(jnp.logical_or(f != t, j != t))
        def _():
            out_copy(j, f).wait_send()

    loop(n_tp, last_out)


def solution(mesh):
    n_fs, n_tp = mesh.shape["fs"], mesh.shape["tp"]

    def local(tokens, mix_heads, norm_first, gate_first, up_first, down_first, out_weight,
              norm_second, gate_second, up_second, down_second):
        rows_in, width = tokens.shape
        total = rows_in * n_fs
        share = total // n_tp
        dc, hidden = gate_first.shape
        heads = mix_heads.shape[1]
        chunk = rows_in // 4
        n_chunks = total // 2 // chunk
        dma = pltpu.SemaphoreType.DMA
        vmem = pl.BlockSpec(memory_space=pltpu.VMEM)
        hbm = pl.BlockSpec(memory_space=pl.ANY)
        return pl.pallas_call(
            functools.partial(kernel, n_fs, n_tp, chunk),
            out_shape=jax.ShapeDtypeStruct((rows_in, width), BF16),
            in_specs=[vmem, vmem, vmem, hbm, hbm, hbm, hbm, vmem, hbm, hbm, hbm],
            out_specs=vmem,
            scratch_shapes=[
                pltpu.VMEM(gate_first.shape, BF16),
                pltpu.VMEM(up_first.shape, BF16),
                pltpu.VMEM(down_first.shape, BF16),
                pltpu.VMEM(out_weight.shape, BF16),
                pltpu.VMEM(gate_second.shape, BF16),
                pltpu.VMEM(up_second.shape, BF16),
                pltpu.VMEM(down_second.shape, BF16),
                pltpu.VMEM((rows_in, width), BF16),
                pltpu.VMEM((rows_in, dc), BF16),
                pltpu.VMEM((total, dc), BF16),
                pltpu.VMEM((total, dc), BF16),
                pltpu.VMEM((total, heads), BF16),
                pltpu.VMEM((2, total, hidden), F32),
                pltpu.VMEM((2, total, hidden), BF16),
                pltpu.VMEM((2, total, hidden), BF16),
                pltpu.VMEM((2, total, hidden), BF16),
                pltpu.VMEM((total, hidden), BF16),
                pltpu.VMEM((total, hidden), BF16),
                pltpu.VMEM((total, dc), BF16),
                pltpu.VMEM((n_tp, share, dc), BF16),
                pltpu.VMEM((n_tp, share, dc), BF16),
                pltpu.VMEM((share, dc), F32),
                pltpu.VMEM((n_fs, 8, share), F32),
                pltpu.VMEM((share, dc), BF16),
                pltpu.VMEM((rows_in, width), BF16),
                dma((7,)), dma((n_fs,)), dma((n_fs,)), dma((n_fs,)), dma,
                dma((n_fs, 2)), dma((n_fs,)),
                dma((2, 2, n_chunks)), dma((2, 2, n_chunks)), dma((2, 2, n_chunks)), dma((2, 2, n_chunks)),
                dma((2, n_tp)), dma((2, n_tp)),
                dma((n_fs,)), dma((n_fs,)), dma((n_tp,)), dma((n_tp,)), dma((n_tp,)), dma((n_fs,)),
            ],
            compiler_params=pltpu.CompilerParams(
                collective_id=0, has_side_effects=True, vmem_limit_bytes=60 * 1024 * 1024),
        )(tokens, mix_heads, norm_first.reshape(1, -1), gate_first, up_first, down_first, out_weight,
          norm_second.reshape(1, -1), gate_second, up_second, down_second)

    in_specs = (
        P(("grp", "fs"), None),
        P(("grp", "fs"), "tp"),
        P(),
        P("fs", "tp"),
        P("fs", "tp"),
        P("tp", "fs"),
        P("tp", "fs"),
        P(),
        P("fs", "tp"),
        P("fs", "tp"),
        P("tp", "fs"),
    )
    return jax.shard_map(local, mesh=mesh, in_specs=in_specs, out_specs=P(("grp", "fs"), None), check_vma=False)
```

time: 764 us -> 213 us (0.28)
  waiting for transfers between devices: 705 us -> 0 us
  Pallas kernels: 0 us -> 211 us
  matrix products: 23.6 us -> 0 us
  blocking collectives: 14.3 us -> 0 us
  between operations: 13.3 us -> 0.01 us
    all_gather x7 -> x0, waiting for transfers between devices: 659 us -> none  [the longest x2 213 us: half_branch(): lax.all_gather(down_weight, 'fs', axis=1, tiled=True)]
    pallas_call x0 -> x1, Pallas kernels: none -> 211 us  [local(): pl.pallas_call(functools.partial(kernel, n_fs, n_tp, chunk), out_shape=ja...]
    reduce_scatter x2 -> x0, waiting for transfers between devices: 41.6 us -> none  [share_sum(): lax.psum_scatter(block_terms.astype(jnp.bfloat16), 'tp', scatter_dimensio...]
    dot_general x5 -> x0, matrix products: 23.6 us -> none  [the longest x2 13.3 us: half_branch(): jnp.dot(hidden, lax.all_gather(down_weight, 'fs', axis=1, tiled=True), pr...]
    all_gather x2 -> x0, blocking collectives: 14.3 us -> none  [join_rows(): return lax.all_gather(row_block, 'tp', axis=0, tiled=True)]
  transfers between devices with their start and end apart: 9 -> 0, of which waited for: 9 -> 0; matrix products, arithmetic and copies ran while one was open for 2% -> 0% of each run, Pallas kernels for 0% -> 0%
where the time goes in v1:
time: 213 us
  Pallas kernels  211 us (99%)
    pallas_call x1, Pallas kernels, local(): pl.pallas_call(functools.partial(kernel, n_fs, n_tp, chunk), out_shape=ja...  211 us

profile of v1, /device:TPU:26, one launch (start us, length us, event | category | flops | bytes accessed | tf_op | source)
XLA Modules:
  0.0 213.2 jit_solution(17637661867020216698)
XLA Ops:
  0.0 211.3 %shard_map.109 = bf16[128,2048]{1,0:T(8,128)(2,1)} custom-call(bf16[128,2048]{1,0:T(8,128)(2,1)} %tok.1, bf16[128,512]{1,0:T(8,128)(2,1)} %mix.1, f32[1,2048]{1,0:T(1,128)} %bitcast.2, bf16[512,1408]{1,0:T(8,128)(2,1)} %wg1.1, bf16[512,1408]{1,0:T(8,128)(2,1)} %wu1.1, bf16[1408,512]{1,0:T(8,128)(2,1)} %wd1.1, bf16[512,512]{1,0:T(8,128)(2,1)} %wo.1, ...), custom_call_target="tpu_custom_call" | custom-call | tf_op jit(solution)/shard_map/pallas_call | solution.py:388
  211.3 1.9 copy.13

commit v2 on v1

v2 whole, which is shorter than its diff:
```python
import functools

import jax
import jax.numpy as jnp
from jax import lax
from jax.experimental import pallas as pl
from jax.experimental.pallas import tpu as pltpu
from jax.sharding import PartitionSpec as P

EPS = 0.1
MESH = pl.DeviceIdType.MESH
BF16 = jnp.bfloat16
F32 = jnp.float32


def loop(count, body):
    def step(i, carry):
        body(i)
        return carry

    lax.fori_loop(0, count, step, 0)


def kernel(n_fs, n_tp, chunk,
           tok, mix, gain1, wg1, wu1, wd1, wo, gain2, wg2, wu2, wd2,
           out,
           vg1, vu1, vd1, vo, vg2, vu2, vd2,
           raw, nb2, mixed, grads, sums, in1, in2, hid1, hid2,
           terms, got1, got2, resid, squares1, squares, done_rows, joined,
           wsem, p0_send, p0_recv, fw_send, fw_recv, s1_send, s1_recv, mix_send, mix_recv,
           rs_send, rs_recv, ag_send, ag_recv, tp_send, tp_recv,
           sq_send, sq_recv, nrm_send, nrm_recv, nfw_send, nfw_recv,
           out_send, out_recv, ofw_send, ofw_recv):
    f, t = lax.axis_index("fs"), lax.axis_index("tp")
    rows_in, width = tok.shape
    total = rows_in * n_fs
    share = total // n_tp
    half = total // 2
    n_chunks = half // chunk
    dc = width // n_fs

    weights = ((wg1, vg1), (wu1, vu1), (wd1, vd1), (wo, vo), (wg2, vg2), (wu2, vu2), (wd2, vd2))
    loads = [pltpu.make_async_copy(a, b, wsem.at[i]) for i, (a, b) in enumerate(weights)]
    for load in loads:
        load.start()

    barrier = pltpu.get_barrier_semaphore()

    def greet(i):
        pf, pt = i // n_tp, i % n_tp

        @pl.when(jnp.logical_or(pf != f, pt != t))
        def _():
            pl.semaphore_signal(barrier, inc=1, device_id={"fs": pf, "tp": pt}, device_id_type=MESH)

    loop(n_fs * n_tp, greet)

    def cols(j):
        return pl.ds(pl.multiple_of(j * dc, dc), dc)

    def block(j, size):
        return pl.ds(pl.multiple_of(j * size, size), size)

    def remote(src, dst, send, recv, **where):
        return pltpu.make_async_remote_copy(
            src_ref=src, dst_ref=dst, send_sem=send, recv_sem=recv,
            device_id=where, device_id_type=MESH)

    c_own = t % 2
    partner = t + 1 - 2 * c_own
    half_in = rows_in // 2
    n_pairs = n_tp // 2

    def squares_of(x):
        own = jnp.sum(x * x, axis=-1, keepdims=True)
        return jnp.transpose(jnp.broadcast_to(own, (x.shape[0], 128)))[0:8, :]

    def scale_of(summed):
        column = jnp.transpose(jnp.broadcast_to(summed[0:1, :], (128, summed.shape[1])))[:, 0:1]
        return lax.rsqrt(column * (1.0 / width) + EPS)

    def piece_of(slot):
        return pl.ds(pl.multiple_of(slot * rows_in + c_own * half_in, half_in), half_in)

    def p0_copy(j, slot):
        return remote(tok.at[block(c_own, half_in), cols(j)], raw.at[piece_of(slot), :],
                      p0_send.at[j], p0_recv.at[slot], fs=j)

    def fw_copy(slot):
        place = raw.at[piece_of(slot), :]
        return remote(place, place, fw_send.at[slot], fw_recv.at[slot], tp=partner)

    def s1_copy(j, slot):
        return remote(squares1.at[f], squares1.at[slot], s1_send.at[j], s1_recv.at[slot], fs=j)

    def sq_copy(j, slot):
        return remote(squares.at[f], squares.at[slot], sq_send.at[j], sq_recv.at[slot], fs=j)

    def mix_copy(slot, side, where):
        place = mixed.at[block(slot, rows_in), :]
        return remote(place, place, mix_send.at[slot, side], mix_recv.at[slot], fs=where)

    mixed[block(f, rows_in), :] = mix[...]
    pl.semaphore_wait(barrier, n_fs * n_tp - 1)

    def p0_start(i):
        p0_copy((f + 1 + i) % n_fs, f).start()

    loop(n_fs - 1, p0_start)
    squares1[f] = squares_of(tok[...].astype(F32))

    def s1_start(i):
        s1_copy((f + 1 + i) % n_fs, f).start()

    loop(n_fs - 1, s1_start)

    @pl.when(f < n_fs - 1)
    def _():
        mix_copy(f, 0, f + 1).start()

    @pl.when(f > 0)
    def _():
        mix_copy(f, 1, f - 1).start()

    raw[block(f, rows_in), :] = tok[:, cols(f)]

    def gates_one(j):
        rows = block(j, rows_in)
        x = (raw[rows, :].astype(F32) * scale_of(squares1[j]) * gain1[:, cols(f)]).astype(BF16)
        grads[0, rows, :] = jnp.dot(x, vg1[...], preferred_element_type=F32)
        grads[1, rows, :] = jnp.dot(x, vu1[...], preferred_element_type=F32)

    def side_of(side):
        hops = jnp.where(side == 0, n_fs - 1 - f, f)
        toward = jnp.where(side == 0, f - 1, f + 1)
        away = jnp.where(side == 0, f + 1, f - 1)
        return hops, toward, away

    near = jnp.where(2 * f >= n_fs, 0, 1)

    def chain(layer, arrived, hid, with_mix):
        def rows_of(side, c):
            return pl.ds(pl.multiple_of(side * half + c * chunk, chunk), chunk)

        def rs_copy(side, c, where):
            rows = rows_of(side, c)
            return remote(sums.at[:, rows, :], arrived.at[:, rows, :],
                          rs_send.at[layer, side, c], rs_recv.at[layer, side, c], fs=where)

        def ag_copy(side, c, where):
            rows = rows_of(side, c)
            return remote(hid.at[rows, :], hid.at[rows, :],
                          ag_send.at[layer, side, c], ag_recv.at[layer, side, c], fs=where)

        for side in (0, 1):
            hops, toward, away = side_of(side)

            @pl.when(hops == 0)
            def _():
                def first(c):
                    rows = rows_of(side, c)
                    sums[:, rows, :] = grads[:, rows, :].astype(BF16)
                    rs_copy(side, c, toward).start()

                loop(n_chunks, first)

        def step(s):
            for k in (0, 1):
                side = near if k == 0 else 1 - near
                hops, toward, away = side_of(side)
                c = s - hops

                @pl.when(jnp.logical_and(hops > 0, jnp.logical_and(c >= 0, c < n_chunks)))
                def _():
                    rows = rows_of(side, c)
                    rs_copy(side, c, f).wait_recv()

                    @pl.when(hops < n_fs - 1)
                    def _():
                        sums[:, rows, :] = (grads[:, rows, :] + arrived[:, rows, :].astype(F32)).astype(BF16)
                        rs_copy(side, c, toward).start()

                    @pl.when(hops == n_fs - 1)
                    def _():
                        g = grads[0, rows, :] + arrived[0, rows, :].astype(F32)
                        v = grads[1, rows, :] + arrived[1, rows, :].astype(F32)
                        hid[rows, :] = (g / (1.0 + jnp.exp(-g)) * v).astype(BF16)
                        ag_copy(side, c, away).start()

            if with_mix:
                @pl.when(jnp.logical_and(s > 0, s < n_fs))
                def _():
                    low, high = f - s, f + s

                    @pl.when(low >= 0)
                    def _():
                        mix_copy(low, 0, f).wait_recv()

                        @pl.when(f < n_fs - 1)
                        def _():
                            mix_copy(low, 0, f + 1).start()

                    @pl.when(high < n_fs)
                    def _():
                        mix_copy(high, 1, f).wait_recv()

                        @pl.when(f > 0)
                        def _():
                            mix_copy(high, 1, f - 1).start()

        loop(n_chunks + n_fs - 1, step)

        def relay(c):
            for k in (0, 1):
                side = 1 - near if k == 0 else near
                hops, toward, away = side_of(side)

                @pl.when(hops < n_fs - 1)
                def _():
                    ag_copy(side, c, f).wait_recv()

                    @pl.when(hops > 0)
                    def _():
                        ag_copy(side, c, away).start()

        def drain(c):
            for side in (0, 1):
                hops, toward, away = side_of(side)

                @pl.when(hops < n_fs - 1)
                def _():
                    rs_copy(side, c, f).wait_send()

                @pl.when(hops > 0)
                def _():
                    ag_copy(side, c, f).wait_send()

        return relay, lambda: loop(n_chunks, drain)

    def tp_copy(layer, j, slot, got):
        return remote(terms.at[block(j, share), :], got.at[slot],
                      tp_send.at[layer, j], tp_recv.at[layer, slot], tp=j)

    def down(layer, relay, hid, vd, got, with_mix):
        per_block = n_chunks // n_pairs

        def piece(b):
            def inner(i):
                relay(b * per_block + i)

            loop(per_block, inner)
            for side in (0, 1):
                j = side * n_pairs + b
                rows = block(j, share)
                value = 0.5 * jnp.dot(hid[rows, :], vd[...], preferred_element_type=F32)
                if with_mix:
                    value = value + jnp.dot(mixed[rows, :], vo[...], preferred_element_type=F32)
                terms[rows, :] = value.astype(BF16)

                @pl.when(j != t)
                def _():
                    tp_copy(layer, j, t, got).start()

        loop(n_pairs, piece)

    def reduce_tp(layer, got, start_value):
        resid[...] = start_value + terms[block(t, share), :].astype(F32)

        def add(i):
            j = (t + 1 + i) % n_tp
            tp_copy(layer, j, j, got).wait_recv()
            resid[...] = resid[...] + got[j].astype(F32)

        loop(n_tp - 1, add)

        def drain(i):
            j = (t + 1 + i) % n_tp
            tp_copy(layer, j, t, got).wait_send()

        loop(n_tp - 1, drain)

    loads[0].wait()
    loads[1].wait()
    gates_one(f)

    def pass_on(i):
        j = (f + 1 + i) % n_fs
        p0_copy(j, j).wait_recv()
        fw_copy(j).start()

    loop(n_fs - 1, pass_on)

    def other_rows(i):
        j = (f + 1 + i) % n_fs
        s1_copy(j, j).wait_recv()
        fw_in(j).wait_recv()
        gates_one(j)

    def fw_in(slot):
        start = pl.multiple_of(slot * rows_in + (1 - c_own) * half_in, half_in)
        place = raw.at[pl.ds(start, half_in), :]
        return remote(place, place, fw_send.at[slot], fw_recv.at[slot], tp=partner)

    loop(n_fs - 1, other_rows)
    relay_one, drain_one = chain(0, in1, hid1, True)
    loads[2].wait()
    loads[3].wait()
    down(0, relay_one, hid1, vd1, got1, True)
    reduce_tp(0, got1, raw[block(t, share), :].astype(F32))

    squares[f] = squares_of(resid[...])

    def sq_start(i):
        sq_copy((f + 1 + i) % n_fs, f).start()

    def sq_wait(i):
        j = (f + 1 + i) % n_fs
        sq_copy(j, j).wait_recv()

    loop(n_fs - 1, sq_start)
    drain_one()
    loop(n_fs - 1, sq_wait)
    summed = squares[0]
    for j in range(1, n_fs):
        summed = summed + squares[j]
    nb2[block(t, share), :] = (resid[...] * scale_of(summed) * gain2[:, cols(f)]).astype(BF16)

    def nrm_copy(j, slot):
        place = nb2.at[block(slot, share), :]
        return remote(place, place, nrm_send.at[j], nrm_recv.at[slot], tp=j)

    def nfw_copy(slot):
        place = nb2.at[block(slot, share), :]
        return remote(place, place, nfw_send.at[slot], nfw_recv.at[slot], tp=partner)

    def same_core(i):
        return (t + 2 + 2 * i) % n_tp

    def nrm_start(i):
        nrm_copy(same_core(i), t).start()

    loop(n_pairs - 1, nrm_start)
    nfw_copy(t).start()
    loads[4].wait()
    loads[5].wait()

    def gates_two(j):
        rows = block(j, share)
        x = nb2[rows, :]
        grads[0, rows, :] = jnp.dot(x, vg2[...], preferred_element_type=F32)
        grads[1, rows, :] = jnp.dot(x, vu2[...], preferred_element_type=F32)

    gates_two(t)
    nfw_copy(partner).wait_recv()
    gates_two(partner)

    def nrm_pass(i):
        j = same_core(i)
        nrm_copy(j, j).wait_recv()
        nfw_copy(j).start()
        gates_two(j)

    loop(n_pairs - 1, nrm_pass)

    def nrm_last(i):
        j = (partner + 2 + 2 * i) % n_tp
        nfw_copy(j).wait_recv()
        gates_two(j)

    loop(n_pairs - 1, nrm_last)
    relay_two, drain_two = chain(1, in2, hid2, False)
    loads[6].wait()
    down(1, relay_two, hid2, vd2, got2, False)
    reduce_tp(1, got2, resid[...])
    done_rows[...] = resid[...].astype(BF16)

    def out_copy(j, slot):
        return remote(done_rows, joined.at[:, cols(slot)], out_send.at[j], out_recv.at[slot], fs=t, tp=j)

    def ofw_copy(slot):
        place = joined.at[:, cols(slot)]
        return remote(place, place, ofw_send.at[slot], ofw_recv.at[slot], tp=partner)

    def out_start(i):
        j = c_own + 2 * i

        @pl.when(jnp.logical_or(f != t, j != t))
        def _():
            out_copy(j, f).start()

    loop(n_pairs, out_start)

    @pl.when(f == t)
    def _():
        joined[:, cols(f)] = done_rows[...]

    takes = c_own == f % 2

    @pl.when(takes)
    def _():
        def take(i):
            j = (f + i) % n_fs

            @pl.when(jnp.logical_or(f != t, j != f))
            def _():
                out_copy(t, j).wait_recv()

            ofw_copy(j).start()

        loop(n_fs, take)

    @pl.when(jnp.logical_not(takes))
    def _():
        def take(i):
            ofw_copy((f + i) % n_fs).wait_recv()

        loop(n_fs, take)

    out[...] = joined[...]

    drain_two()

    def last_fs(i):
        j = (f + 1 + i) % n_fs
        p0_copy(j, f).wait_send()
        fw_copy(j).wait_send()
        s1_copy(j, f).wait_send()
        sq_copy(j, f).wait_send()

    loop(n_fs - 1, last_fs)

    def last_mix(j):
        @pl.when(jnp.logical_and(j <= f, f < n_fs - 1))
        def _():
            mix_copy(j, 0, f).wait_send()

        @pl.when(jnp.logical_and(j >= f, f > 0))
        def _():
            mix_copy(j, 1, f).wait_send()

        @pl.when(takes)
        def _():
            ofw_copy(j).wait_send()

    loop(n_fs, last_mix)

    def last_nrm(i):
        nrm_copy(same_core(i), t).wait_send()

    loop(n_pairs - 1, last_nrm)

    def last_out(i):
        j = c_own + 2 * i
        nfw_copy(j).wait_send()

        @pl.when(jnp.logical_or(f != t, j != t))
        def _():
            out_copy(j, f).wait_send()

    loop(n_pairs, last_out)


def solution(mesh):
    n_fs, n_tp = mesh.shape["fs"], mesh.shape["tp"]

    def local(tokens, mix_heads, norm_first, gate_first, up_first, down_first, out_weight,
              norm_second, gate_second, up_second, down_second):
        rows_in, width = tokens.shape
        total = rows_in * n_fs
        share = total // n_tp
        dc, hidden = gate_first.shape
        heads = mix_heads.shape[1]
        chunk = rows_in // 4
        n_chunks = total // 2 // chunk
        dma = pltpu.SemaphoreType.DMA
        vmem = pl.BlockSpec(memory_space=pltpu.VMEM)
        hbm = pl.BlockSpec(memory_space=pl.ANY)
        return pl.pallas_call(
            functools.partial(kernel, n_fs, n_tp, chunk),
            out_shape=jax.ShapeDtypeStruct((rows_in, width), BF16),
            in_specs=[vmem, vmem, vmem, hbm, hbm, hbm, hbm, vmem, hbm, hbm, hbm],
            out_specs=vmem,
            scratch_shapes=[
                pltpu.VMEM(gate_first.shape, BF16),
                pltpu.VMEM(up_first.shape, BF16),
                pltpu.VMEM(down_first.shape, BF16),
                pltpu.VMEM(out_weight.shape, BF16),
                pltpu.VMEM(gate_second.shape, BF16),
                pltpu.VMEM(up_second.shape, BF16),
                pltpu.VMEM(down_second.shape, BF16),
                pltpu.VMEM((total, dc), BF16),
                pltpu.VMEM((total, dc), BF16),
                pltpu.VMEM((total, heads), BF16),
                pltpu.VMEM((2, total, hidden), F32),
                pltpu.VMEM((2, total, hidden), BF16),
                pltpu.VMEM((2, total, hidden), BF16),
                pltpu.VMEM((2, total, hidden), BF16),
                pltpu.VMEM((total, hidden), BF16),
                pltpu.VMEM((total, hidden), BF16),
                pltpu.VMEM((total, dc), BF16),
                pltpu.VMEM((n_tp, share, dc), BF16),
                pltpu.VMEM((n_tp, share, dc), BF16),
                pltpu.VMEM((share, dc), F32),
                pltpu.VMEM((n_fs, 8, rows_in), F32),
                pltpu.VMEM((n_fs, 8, share), F32),
                pltpu.VMEM((share, dc), BF16),
                pltpu.VMEM((rows_in, width), BF16),
                dma((7,)), dma((n_fs,)), dma((n_fs,)), dma((n_fs,)), dma((n_fs,)), dma((n_fs,)), dma((n_fs,)),
                dma((n_fs, 2)), dma((n_fs,)),
                dma((2, 2, n_chunks)), dma((2, 2, n_chunks)), dma((2, 2, n_chunks)), dma((2, 2, n_chunks)),
                dma((2, n_tp)), dma((2, n_tp)),
                dma((n_fs,)), dma((n_fs,)), dma((n_tp,)), dma((n_tp,)), dma((n_tp,)), dma((n_tp,)),
                dma((n_tp,)), dma((n_fs,)), dma((n_fs,)), dma((n_fs,)),
            ],
            compiler_params=pltpu.CompilerParams(
                collective_id=0, has_side_effects=True, vmem_limit_bytes=60 * 1024 * 1024),
        )(tokens, mix_heads, norm_first.reshape(1, -1), gate_first, up_first, down_first, out_weight,
          norm_second.reshape(1, -1), gate_second, up_second, down_second)

    in_specs = (
        P(("grp", "fs"), None),
        P(("grp", "fs"), "tp"),
        P(),
        P("fs", "tp"),
        P("fs", "tp"),
        P("tp", "fs"),
        P("tp", "fs"),
        P(),
        P("fs", "tp"),
        P("fs", "tp"),
        P("tp", "fs"),
    )
    return jax.shard_map(local, mesh=mesh, in_specs=in_specs, out_specs=P(("grp", "fs"), None), check_vma=False)
```

time: 213 us -> 201 us (0.944); the launches traced: 213 us -> 198 us
  Pallas kernels: 211 us -> 196 us
    pallas_call x1, Pallas kernels: 211 us -> 196 us  [local(): pl.pallas_call(functools.partial(kernel, n_fs, n_tp, chunk), out_shape=ja...]
where the time goes in v2:
time: 201 us; the launch traced here: 198 us
  Pallas kernels  196 us (98%)
    pallas_call x1, Pallas kernels, local(): pl.pallas_call(functools.partial(kernel, n_fs, n_tp, chunk), out_shape=ja...  196 us

profile of v2, /device:TPU:26, one launch (start us, length us, event | category | flops | bytes accessed | tf_op | source)
XLA Modules:
  0.0 198.3 jit_solution(3743797999149833586)
XLA Ops:
  0.0 196.4 %shard_map.109 = bf16[128,2048]{1,0:T(8,128)(2,1)} custom-call(bf16[128,2048]{1,0:T(8,128)(2,1)} %tok.1, bf16[128,512]{1,0:T(8,128)(2,1)} %mix.1, f32[1,2048]{1,0:T(1,128)} %bitcast.2, bf16[512,1408]{1,0:T(8,128)(2,1)} %wg1.1, bf16[512,1408]{1,0:T(8,128)(2,1)} %wu1.1, bf16[1408,512]{1,0:T(8,128)(2,1)} %wd1.1, bf16[512,512]{1,0:T(8,128)(2,1)} %wo.1, ...), custom_call_target="tpu_custom_call" | custom-call | tf_op jit(solution)/shard_map/pallas_call | solution.py:478
  196.4 1.9 copy.13

commit v3 on v2

--- a/solution.py
+++ b/solution.py
@@ -470,7 +470,7 @@
         share = total // n_tp
         dc, hidden = gate_first.shape
         heads = mix_heads.shape[1]
-        chunk = rows_in // 4
+        chunk = rows_in // 2
         n_chunks = total // 2 // chunk
         dma = pltpu.SemaphoreType.DMA
         vmem = pl.BlockSpec(memory_space=pltpu.VMEM)

time: 201 us -> 187 us (0.930)
  Pallas kernels: 196 us -> 182 us
    pallas_call x1, Pallas kernels: 196 us -> 182 us  [local(): pl.pallas_call(functools.partial(kernel, n_fs, n_tp, chunk), out_shape=ja...]
where the time goes in v3:
time: 187 us; the launch traced here: 184 us
  Pallas kernels  182 us (97%)
  local copies, waits for them, and re-layouts  1.88 us (1%)
    pallas_call x1, Pallas kernels, local(): pl.pallas_call(functools.partial(kernel, n_fs, n_tp, chunk), out_shape=ja...  182 us

profile of v3, /device:TPU:26, one launch (start us, length us, event | category | flops | bytes accessed | tf_op | source)
XLA Modules:
  0.0 183.9 jit_solution(4681555206822394491)
XLA Ops:
  0.0 182.0 %shard_map.109 = bf16[128,2048]{1,0:T(8,128)(2,1)} custom-call(bf16[128,2048]{1,0:T(8,128)(2,1)} %tok.1, bf16[128,512]{1,0:T(8,128)(2,1)} %mix.1, f32[1,2048]{1,0:T(1,128)} %bitcast.2, bf16[512,1408]{1,0:T(8,128)(2,1)} %wg1.1, bf16[512,1408]{1,0:T(8,128)(2,1)} %wu1.1, bf16[1408,512]{1,0:T(8,128)(2,1)} %wd1.1, bf16[512,512]{1,0:T(8,128)(2,1)} %wo.1, ...), custom_call_target="tpu_custom_call" | custom-call | tf_op jit(solution)/shard_map/pallas_call | solution.py:478
  182.0 1.9 %copy.13 = bf16[128,2048]{1,0:T(8,128)(2,1)} copy(bf16[128,2048]{1,0:T(8,128)(2,1)} %shard_map.109) | data formatting | bytes 1048576

commit v4 on v3

--- a/solution.py
+++ b/solution.py
@@ -26,11 +26,11 @@
            out,
            vg1, vu1, vd1, vo, vg2, vu2, vd2,
            raw, nb2, mixed, grads, sums, in1, in2, hid1, hid2,
-           terms, got1, got2, resid, squares1, squares, done_rows, joined,
+           terms, got1, got2, resid, squares1, squares1_in, squares, done_rows, joined,
            wsem, p0_send, p0_recv, fw_send, fw_recv, s1_send, s1_recv, mix_send, mix_recv,
            rs_send, rs_recv, ag_send, ag_recv, tp_send, tp_recv,
            sq_send, sq_recv, nrm_send, nrm_recv, nfw_send, nfw_recv,
-           out_send, out_recv, ofw_send, ofw_recv):
+           out_send, out_recv, ofw_send, ofw_recv, sfw_send, sfw_recv):
     f, t = lax.axis_index("fs"), lax.axis_index("tp")
     rows_in, width = tok.shape
     total = rows_in * n_fs
@@ -110,7 +110,11 @@
     squares1[f] = squares_of(tok[...].astype(F32))
 
     def s1_start(i):
-        s1_copy((f + 1 + i) % n_fs, f).start()
+        j = (f + 1 + i) % n_fs
+
+        @pl.when(j % 2 == c_own)
+        def _():
+            s1_copy(j, f).start()
 
     loop(n_fs - 1, s1_start)
 
@@ -124,9 +128,9 @@
 
     raw[block(f, rows_in), :] = tok[:, cols(f)]
 
-    def gates_one(j):
+    def gates_one(j, sums_of):
         rows = block(j, rows_in)
-        x = (raw[rows, :].astype(F32) * scale_of(squares1[j]) * gain1[:, cols(f)]).astype(BF16)
+        x = (raw[rows, :].astype(F32) * scale_of(sums_of[j]) * gain1[:, cols(f)]).astype(BF16)
         grads[0, rows, :] = jnp.dot(x, vg1[...], preferred_element_type=F32)
         grads[1, rows, :] = jnp.dot(x, vu1[...], preferred_element_type=F32)
 
@@ -281,7 +285,7 @@
 
     loads[0].wait()
     loads[1].wait()
-    gates_one(f)
+    gates_one(f, squares1)
 
     def pass_on(i):
         j = (f + 1 + i) % n_fs
@@ -290,11 +294,27 @@
 
     loop(n_fs - 1, pass_on)
 
+    takes = c_own == f % 2
+    share_sums = remote(squares1, squares1_in, sfw_send, sfw_recv, tp=partner)
+
+    @pl.when(takes)
+    def _():
+        def take_sums(i):
+            j = (f + 1 + i) % n_fs
+            s1_copy(j, j).wait_recv()
+
+        loop(n_fs - 1, take_sums)
+        share_sums.start()
+        squares1_in[...] = squares1[...]
+
+    @pl.when(jnp.logical_not(takes))
+    def _():
+        share_sums.wait_recv()
+
     def other_rows(i):
         j = (f + 1 + i) % n_fs
-        s1_copy(j, j).wait_recv()
         fw_in(j).wait_recv()
-        gates_one(j)
+        gates_one(j, squares1_in)
 
     def fw_in(slot):
         start = pl.multiple_of(slot * rows_in + (1 - c_own) * half_in, half_in)
@@ -394,8 +414,6 @@
     def _():
         joined[:, cols(f)] = done_rows[...]
 
-    takes = c_own == f % 2
-
     @pl.when(takes)
     def _():
         def take(i):
@@ -424,10 +442,18 @@
         j = (f + 1 + i) % n_fs
         p0_copy(j, f).wait_send()
         fw_copy(j).wait_send()
-        s1_copy(j, f).wait_send()
+
+        @pl.when(j % 2 == c_own)
+        def _():
+            s1_copy(j, f).wait_send()
+
         sq_copy(j, f).wait_send()
 
     loop(n_fs - 1, last_fs)
+
+    @pl.when(takes)
+    def _():
+        share_sums.wait_send()
 
     def last_mix(j):
         @pl.when(jnp.logical_and(j <= f, f < n_fs - 1))
@@ -502,6 +528,7 @@
                 pltpu.VMEM((n_tp, share, dc), BF16),
                 pltpu.VMEM((share, dc), F32),
                 pltpu.VMEM((n_fs, 8, rows_in), F32),
+                pltpu.VMEM((n_fs, 8, rows_in), F32),
                 pltpu.VMEM((n_fs, 8, share), F32),
                 pltpu.VMEM((share, dc), BF16),
                 pltpu.VMEM((rows_in, width), BF16),
@@ -510,7 +537,7 @@
                 dma((2, 2, n_chunks)), dma((2, 2, n_chunks)), dma((2, 2, n_chunks)), dma((2, 2, n_chunks)),
                 dma((2, n_tp)), dma((2, n_tp)),
                 dma((n_fs,)), dma((n_fs,)), dma((n_tp,)), dma((n_tp,)), dma((n_tp,)), dma((n_tp,)),
-                dma((n_tp,)), dma((n_fs,)), dma((n_fs,)), dma((n_fs,)),
+                dma((n_tp,)), dma((n_fs,)), dma((n_fs,)), dma((n_fs,)), dma, dma,
             ],
             compiler_params=pltpu.CompilerParams(
                 collective_id=0, has_side_effects=True, vmem_limit_bytes=60 * 1024 * 1024),

time: 187 us -> 188 us (level)
  Pallas kernels: 182 us -> 184 us
    pallas_call x1, Pallas kernels: 182 us -> 184 us  [local(): pl.pallas_call(functools.partial(kernel, n_fs, n_tp, chunk), out_shape=ja...]
where the time goes in v4:
time: 188 us; the launch traced here: 186 us
  Pallas kernels  184 us (98%)
    pallas_call x1, Pallas kernels, local(): pl.pallas_call(functools.partial(kernel, n_fs, n_tp, chunk), out_shape=ja...  184 us

profile of v4, /device:TPU:26, one launch (start us, length us, event | category | flops | bytes accessed | tf_op | source)
XLA Modules:
  0.0 186.1 jit_solution(4246798807773819915)
XLA Ops:
  0.0 184.2 %shard_map.109 = bf16[128,2048]{1,0:T(8,128)(2,1)} custom-call(bf16[128,2048]{1,0:T(8,128)(2,1)} %tok.1, bf16[128,512]{1,0:T(8,128)(2,1)} %mix.1, f32[1,2048]{1,0:T(1,128)} %bitcast.2, bf16[512,1408]{1,0:T(8,128)(2,1)} %wg1.1, bf16[512,1408]{1,0:T(8,128)(2,1)} %wu1.1, bf16[1408,512]{1,0:T(8,128)(2,1)} %wd1.1, bf16[512,512]{1,0:T(8,128)(2,1)} %wo.1, ...), custom_call_target="tpu_custom_call" | custom-call | tf_op jit(solution)/shard_map/pallas_call | solution.py:504
  184.2 1.9 %copy.13 = bf16[128,2048]{1,0:T(8,128)(2,1)} copy(bf16[128,2048]{1,0:T(8,128)(2,1)} %shard_map.109) | data formatting | bytes 1048576

commit v5 on v3

--- a/solution.py
+++ b/solution.py
@@ -114,12 +114,9 @@
 
     loop(n_fs - 1, s1_start)
 
-    @pl.when(f < n_fs - 1)
+    @pl.when(jnp.logical_and(f > 0, f < n_fs - 1))
     def _():
         mix_copy(f, 0, f + 1).start()
-
-    @pl.when(f > 0)
-    def _():
         mix_copy(f, 1, f - 1).start()
 
     raw[block(f, rows_in), :] = tok[:, cols(f)]
@@ -163,6 +160,8 @@
                     rs_copy(side, c, toward).start()
 
                 loop(n_chunks, first)
+                if with_mix:
+                    mix_copy(f, 1 - side, toward).start()
 
         def step(s):
             for k in (0, 1):
@@ -187,28 +186,31 @@
                         hid[rows, :] = (g / (1.0 + jnp.exp(-g)) * v).astype(BF16)
                         ag_copy(side, c, away).start()
 
-            if with_mix:
-                @pl.when(jnp.logical_and(s > 0, s < n_fs))
-                def _():
-                    low, high = f - s, f + s
-
-                    @pl.when(low >= 0)
+        loop(n_chunks + n_fs - 1, step)
+
+        def mix_step(s):
+            @pl.when(jnp.logical_and(s > 0, s < n_fs))
+            def _():
+                low, high = f - s, f + s
+
+                @pl.when(low >= 0)
+                def _():
+                    mix_copy(low, 0, f).wait_recv()
+
+                    @pl.when(f < n_fs - 1)
                     def _():
-                        mix_copy(low, 0, f).wait_recv()
-
-                        @pl.when(f < n_fs - 1)
-                        def _():
-                            mix_copy(low, 0, f + 1).start()
-
-                    @pl.when(high < n_fs)
+                        mix_copy(low, 0, f + 1).start()
+
+                @pl.when(high < n_fs)
+                def _():
+                    mix_copy(high, 1, f).wait_recv()
+
+                    @pl.when(f > 0)
                     def _():
-                        mix_copy(high, 1, f).wait_recv()
-
-                        @pl.when(f > 0)
-                        def _():
-                            mix_copy(high, 1, f - 1).start()
-
-        loop(n_chunks + n_fs - 1, step)
+                        mix_copy(high, 1, f - 1).start()
+
+        if with_mix:
+            loop(n_fs, mix_step)
 
         def relay(c):
             for k in (0, 1):

time: 187 us -> 190 us (1.016)
  Pallas kernels: 182 us -> 187 us
    pallas_call x1, Pallas kernels: 182 us -> 187 us  [local(): pl.pallas_call(functools.partial(kernel, n_fs, n_tp, chunk), out_shape=ja...]
where the time goes in v5:
time: 190 us; the launch traced here: 188 us
  Pallas kernels  187 us (98%)
    pallas_call x1, Pallas kernels, local(): pl.pallas_call(functools.partial(kernel, n_fs, n_tp, chunk), out_shape=ja...  187 us

profile of v5, /device:TPU:26, one launch (start us, length us, event | category | flops | bytes accessed | tf_op | source)
XLA Modules:
  0.0 188.4 jit_solution(502220306892085349)
XLA Ops:
  0.0 186.5 %shard_map.109 = bf16[128,2048]{1,0:T(8,128)(2,1)} custom-call(bf16[128,2048]{1,0:T(8,128)(2,1)} %tok.1, bf16[128,512]{1,0:T(8,128)(2,1)} %mix.1, f32[1,2048]{1,0:T(1,128)} %bitcast.2, bf16[512,1408]{1,0:T(8,128)(2,1)} %wg1.1, bf16[512,1408]{1,0:T(8,128)(2,1)} %wu1.1, bf16[1408,512]{1,0:T(8,128)(2,1)} %wd1.1, bf16[512,512]{1,0:T(8,128)(2,1)} %wo.1, ...), custom_call_target="tpu_custom_call" | custom-call | tf_op jit(solution)/shard_map/pallas_call | solution.py:480
  186.6 1.9 copy.13
